TPU v7x, 32 devices: a whole 2x2x4 slice. The times are simulated.
32 devices in a mesh: fs: 4 (over y, x), tp: 8 (over z, core).
Axes of the slice: x: 2, y: 2, z: 4, core: 2. Of those that a mesh axis runs over, the one named last changes fastest.
Arguments:
- inputs: bfloat16 [8, 320, 2048], P('tp'), may hold values from -6 to 6
- cotangent: bfloat16 [8, 320, 2048], P('tp'), may hold values from -8 to 8
- gate_weight: bfloat16 [2048, 5632], P('tp', 'fs'), may hold values from -0.125 to 0.125
- up_weight: bfloat16 [2048, 5632], P('tp', 'fs'), may hold values from -0.125 to 0.125
- down_weight: bfloat16 [5632, 2048], P('fs', 'tp'), may hold values from -0.078125 to 0.078125
Outputs:
- input_grad: bfloat16 [8, 320, 2048], P('tp')
- down_grad: float32 [5632, 2048], P('fs', 'tp')
All inputs are finite; a program needn't handle non-finite values.
Results may differ from a plain program's by a relative error of at most 0.023.
Values may be sent and summed in bfloat16 or wider, within the bound.
A program may use at most 64 MiB of HBM per device.

v0:
```python
import jax
import jax.numpy as jnp
from jax import lax
from jax.sharding import PartitionSpec as P


def contract_hidden(left, right):
    return lax.dot_general(
        left, right, (((1,), (1,)), ((), ())), preferred_element_type=jnp.float32
    )


def contract_tokens(left, right):
    return lax.dot_general(
        left, right, (((0,), (0,)), ((), ())), preferred_element_type=jnp.float32
    )


def per_device(inputs, cotangent, gate_weight, up_weight, down_weight):
    rows_in = inputs[0]
    rows_grad = cotangent[0]
    token_count = rows_in.shape[0]
    model_width = rows_in.shape[1]
    gate_full, up_full, down_tall = (
        lax.all_gather(gate_weight, "tp", axis=0, tiled=True),
        lax.all_gather(up_weight, "tp", axis=0, tiled=True),
        lax.all_gather(down_weight.T, "tp", axis=0, tiled=True),
    )
    gate_pre = jnp.dot(rows_in, gate_full, preferred_element_type=jnp.float32)
    up_pre = jnp.dot(rows_in, up_full, preferred_element_type=jnp.float32)
    sig = jax.nn.sigmoid(gate_pre)
    hidden = (gate_pre * sig * up_pre).astype(jnp.bfloat16)
    hidden_grad = jnp.dot(rows_grad, down_tall, preferred_element_type=jnp.float32)
    gate_grad = (hidden_grad * up_pre * sig * (1.0 + gate_pre * (1.0 - sig))).astype(jnp.bfloat16)
    up_grad = (hidden_grad * gate_pre * sig).astype(jnp.bfloat16)
    partial_down = contract_tokens(hidden, rows_grad)
    down_grad = lax.psum_scatter(
        partial_down.astype(jnp.bfloat16), "tp", scatter_dimension=1, tiled=True
    ).astype(jnp.float32)
    own_sum = lax.psum_scatter(
        (contract_hidden(gate_grad, gate_full) + contract_hidden(up_grad, up_full)).astype(
            jnp.bfloat16
        ),
        "fs",
        scatter_dimension=0,
        tiled=True,
    )
    whole_grad = lax.all_gather(own_sum, "fs", axis=0, tiled=True)
    input_grad = whole_grad.reshape(1, token_count, model_width)
    return (input_grad, down_grad)


def solution(mesh):
    return jax.shard_map(
        per_device,
        mesh=mesh,
        in_specs=(
            P("tp", None, None),
            P("tp", None, None),
            P("tp", "fs"),
            P("tp", "fs"),
            P("fs", "tp"),
        ),
        out_specs=(P("tp", None, None), P("fs", "tp")),
        check_vma=False,
    )
```

profile of v0, /device:TPU:0, one launch (start us, length us, event | category | flops | bytes accessed | tf_op | source)
XLA Modules:
  0.0 342.6 jit_solution(16475560544088254756)
XLA Ops:
  7.2 0.0 copy-start
  7.2 0.0 all-gather.9.cloned.1.call-start
  7.2 0.7 all-gather.9.cloned.1.call-update
  7.9 0.0 all-gather.7.cloned.1.call-start
  8.0 0.7 all-gather.7.cloned.1.call-update
  8.7 0.0 all-gather.5.cloned.1.call-start
  8.7 0.7 all-gather.5.cloned.1.call-update
  9.4 0.0 reduce-scatter.3.cloned.1.call-start
  9.5 63.3 %all-gather.9.cloned.1.call-done = bf16[2048,1408]{1,0:T(8,128)(2,1)} async-done(((bf16[256,1408]{1,0:T(8,128)(2,1)}), bf16[2048,1408]{1,0:T(8,128)(2,1)}) %all-gather.9.cloned.1.call-update) | async-done | bytes 5767184 | tf_op jit(solution)/shard_map/all_gather | solution.py:25
  72.8 0.0 copy-done.3
  72.8 6.1 %fusion.1 = f32[320,1408]{1,0:T(8,128)} fusion(bf16[2048,1408]{1,0:T(8,128)(2,1)} %all-gather.9.cloned.1.call-done, bf16[1,320,2048]{2,1,0:T(8,128)(2,1)S(1)} %copy-done.3), kind=kOutput, calls=%fused_computation.7 | convolution fusion | flops 1845493760 | bytes 8880128 | tf_op jit(solution)/shard_map/dot_general | solution.py:29
  78.8 54.6 %all-gather.7.cloned.1.call-done = bf16[2048,1408]{1,0:T(8,128)(2,1)} async-done(((bf16[256,1408]{1,0:T(8,128)(2,1)}), bf16[2048,1408]{1,0:T(8,128)(2,1)}) %all-gather.7.cloned.1.call-update) | async-done | bytes 5767184 | tf_op jit(solution)/shard_map/all_gather | solution.py:26
  133.5 6.1 %fusion.3 = f32[320,1408]{1,0:T(8,128)} fusion(bf16[2048,1408]{1,0:T(8,128)(2,1)} %all-gather.7.cloned.1.call-done, bf16[1,320,2048]{2,1,0:T(8,128)(2,1)S(1)} %copy-done.3), kind=kOutput, calls=%fused_computation.9 | convolution fusion | flops 1845493760 | bytes 8880128 | tf_op jit(solution)/shard_map/dot_general | solution.py:30
  139.6 55.0 %all-gather.5.cloned.1.call-done = bf16[2048,1408]{0,1:T(8,128)(2,1)} async-done(((bf16[256,1408]{0,1:T(8,128)(2,1)}), bf16[2048,1408]{0,1:T(8,128)(2,1)}) %all-gather.5.cloned.1.call-update) | async-done | bytes 5767184 | tf_op jit(solution)/shard_map/all_gather | solution.py:27
  194.6 5.0 %fusion.6 = f32[320,1408]{1,0:T(8,128)S(1)} fusion(bf16[2048,1408]{0,1:T(8,128)(2,1)} %all-gather.5.cloned.1.call-done, bf16[1,320,2048]{2,1,0:T(8,128)(2,1)S(1)} %copy-done), kind=kOutput, calls=%fused_computation.12 | convolution fusion | flops 1845493760 | bytes 8880128 | tf_op jit(solution)/shard_map/dot_general | solution.py:33
  199.6 0.0 copy-done.4
  199.6 0.0 copy-done.2
  199.6 0.0 slice-start.1
  199.6 4.1 %fusion.8 = f32[320,2048]{1,0:T(8,128)S(1)} fusion(bf16[2048,1408]{1,0:T(8,128)(2,1)S(1)} %copy-done.2, f32[320,1408]{1,0:T(8,128)S(1)} %copy-done.4, f32[320,1408]{1,0:T(8,128)S(1)} %fusion.6, f32[320,1408]{1,0:T(8,128)} %fusion.3), kind=kOutput, calls=%fused_computation.14 | convolution fusion | flops 1849999360 | bytes 13795328 | tf_op jit(solution)/shard_map/dot_general | solution.py:8
  203.8 0.0 slice-done
  203.8 3.4 fusion
  207.2 0.0 reduce-scatter.3.cloned.1.call-update
  207.2 0.0 all-gather.11.cloned.1.call-start
  207.3 27.8 %reduce-scatter.3.cloned.1.call-done = bf16[80,2048]{1,0:T(8,128)(2,1)} async-done(((bf16[320,2048]{1,0:T(8,128)(2,1)}), bf16[80,2048]{1,0:T(8,128)(2,1)}) %reduce-scatter.3.cloned.1.call-update) | async-done | bytes 327696 | tf_op jit(solution)/shard_map/reduce_scatter | solution.py:40
  235.0 0.0 all-gather.11.cloned.1.call-update
  235.1 0.0 reduce-scatter.5.cloned.1.call-start
  235.1 6.7 %convolution_convert_fusion = bf16[1408,2048]{1,0:T(8,128)(2,1)} fusion(bf16[1,320,2048]{2,1,0:T(8,128)(2,1)S(1)} %copy-done, f32[320,1408]{1,0:T(8,128)} %fusion.3, f32[320,1408]{1,0:T(8,128)S(1)} %copy-done.4), kind=kOutput, calls=%fused_computation | convolution fusion | flops 1851080704 | bytes 10682368 | tf_op jit(solution)/shard_map/dot_general | solution.py:14
  241.8 0.0 reduce-scatter.5.cloned.1.call-update
  241.8 23.6 %all-gather.11.cloned.1.call-done = bf16[320,2048]{1,0:T(8,128)(2,1)} async-done(((bf16[80,2048]{1,0:T(8,128)(2,1)}), bf16[320,2048]{1,0:T(8,128)(2,1)}) %all-gather.11.cloned.1.call-update) | async-done | bytes 1310736 | tf_op jit(solution)/shard_map/all_gather | solution.py:48
  265.4 67.0 %reduce-scatter.5.cloned.1.call-done = bf16[1408,256]{1,0:T(8,128)(2,1)} async-done(((bf16[1408,2048]{1,0:T(8,128)(2,1)}), bf16[1408,256]{1,0:T(8,128)(2,1)}) %reduce-scatter.5.cloned.1.call-update) | async-done | bytes 720912 | tf_op jit(solution)/shard_map/reduce_scatter | solution.py:37
  332.4 2.3 convert_element_type.23
  334.7 1.1 copy.8
  (9 shorter events, 0.0 us)
Async XLA Ops:
  7.2 187.4 %copy-start = (bf16[1,320,2048]{2,1,0:T(8,128)(2,1)S(1)}, bf16[1,320,2048]{2,1,0:T(8,128)(2,1)}, u32[]{:S(2)}) copy-start(bf16[1,320,2048]{2,1,0:T(8,128)(2,1)} %param.6) | copy-start | bytes 3932164
  7.2 65.6 %copy-start.3 = (bf16[1,320,2048]{2,1,0:T(8,128)(2,1)S(1)}, bf16[1,320,2048]{2,1,0:T(8,128)(2,1)}, u32[]{:S(2)}) copy-start(bf16[1,320,2048]{2,1,0:T(8,128)(2,1)} %param.5) | copy-start | bytes 3932164
  7.2 65.6 %all-gather.9.cloned.1.call-start = ((), (), s32[]{:S(2)}) async-start(), calls=%async_computation.4 | async-start | bytes 6488064 | tf_op jit(solution)/shard_map/all_gather | solution.py:25
  7.9 125.5 %all-gather.7.cloned.1.call-start = ((), (), s32[]{:S(2)}) async-start(), calls=%async_computation.3 | async-start | bytes 6488064 | tf_op jit(solution)/shard_map/all_gather | solution.py:26
  8.7 185.9 %all-gather.5.cloned.1.call-start = ((), (), s32[]{:S(2)}) async-start(), calls=%async_computation.2 | async-start | bytes 6488064 | tf_op jit(solution)/shard_map/all_gather | solution.py:27
  9.4 225.6 %reduce-scatter.3.cloned.1.call-start = ((), (), s32[]{:S(2)}) async-start(), calls=%async_computation.5 | async-start | bytes 1638400 | tf_op jit(solution)/shard_map/reduce_scatter | solution.py:40
  139.6 60.1 %copy-start.4 = (f32[320,1408]{1,0:T(8,128)S(1)}, f32[320,1408]{1,0:T(8,128)}, u32[]{:S(2)}) copy-start(f32[320,1408]{1,0:T(8,128)} %fusion.1) | copy-start | bytes 5406724
  194.6 5.0 %copy-start.2 = (bf16[2048,1408]{1,0:T(8,128)(2,1)S(1)}, bf16[2048,1408]{1,0:T(8,128)(2,1)}, u32[]{:S(2)}) copy-start(bf16[2048,1408]{1,0:T(8,128)(2,1)} %all-gather.9.cloned.1.call-done) | copy-start | bytes 17301508
  194.6 9.2 %slice-start = ((s8[5767168]{0:T(1024)(128)(4,1)}), s8[4194304]{0:T(1024)(128)(4,1)S(1)}, s32[]{:S(2)}) async-start(s8[5767168]{0:T(1024)(128)(4,1)} %bitcast.19), calls=%async_computation.8 | async-start | bytes 8388608
  199.6 4.2 %slice-start.1 = ((s8[5767168]{0:T(1024)(128)(4,1)}), s8[1572864]{0:T(1024)(128)(4,1)S(1)}, s32[]{:S(2)}) async-start(s8[5767168]{0:T(1024)(128)(4,1)} %bitcast.19), calls=%async_computation.9 | async-start | bytes 3145728
  207.2 58.2 %all-gather.11.cloned.1.call-start = ((), (), s32[]{:S(2)}) async-start(), calls=%async_computation.6 | async-start | bytes 1638400 | tf_op jit(solution)/shard_map/all_gather | solution.py:48
  235.1 97.3 %reduce-scatter.5.cloned.1.call-start = ((), (), s32[]{:S(2)}) async-start(), calls=%async_computation.7 | async-start | bytes 6488064 | tf_op jit(solution)/shard_map/reduce_scatter | solution.py:37
  265.4 69.3 %copy-start.1 = (bf16[320,2048]{1,0:T(8,128)(2,1)S(1)}, bf16[320,2048]{1,0:T(8,128)(2,1)}, u32[]{:S(2)}) copy-start(bf16[320,2048]{1,0:T(8,128)(2,1)} %all-gather.11.cloned.1.call-done) | copy-start | bytes 3932164
Sparse Core Ops, SparseCore 0:
  9.6 63.0 all-gather.8
  74.4 59.0 all-gather.6
  135.1 59.4 all-gather.4
  207.3 27.6 reduce-scatter.2
  236.7 28.6 all-gather.10
  267.6 64.7 reduce-scatter.4
where the time goes:
time: 343 us
  waiting for transfers between devices  293 us (85%)
  matrix products  31.3 us (9%)
  between operations  14.2 us (4%)
    reduce_scatter x1, waiting for transfers between devices, per_device(): lax.psum_scatter(partial_down.astype(jnp.bfloat16), 'tp', scatter_dimensi...  67 us
    all_gather x1, waiting for transfers between devices, per_device(): lax.all_gather(gate_weight, 'tp', axis=0, tiled=True)  63.3 us
    all_gather x1, waiting for transfers between devices, per_device(): lax.all_gather(down_weight.T, 'tp', axis=0, tiled=True)  55 us
    all_gather x1, waiting for transfers between devices, per_device(): lax.all_gather(up_weight, 'tp', axis=0, tiled=True)  54.6 us
    reduce_scatter x1, waiting for transfers between devices, per_device(): lax.psum_scatter((contract_hidden(gate_grad, gate_full) + contract_hidden...  27.8 us
    all_gather x1, waiting for transfers between devices, per_device(): whole_grad = lax.all_gather(own_sum, 'fs', axis=0, tiled=True)  23.6 us
    dot_general x2, matrix products, contract_hidden(): lax.dot_general(left, right, (((1,), (1,)), ((), ())), preferred_element_...  7.51 us
  transfers between devices with their start and end apart: 6, of which 6 were waited for; matrix products, arithmetic and copies ran while one was open for 5% of the time, Pallas kernels for 0%

commit v1 on v0

--- a/solution.py
+++ b/solution.py
@@ -23,7 +23,9 @@
     model_width = rows_in.shape[1]
     gate_full, up_full, down_tall = (
         lax.all_gather(gate_weight, "tp", axis=0, tiled=True),
-        lax.all_gather(up_weight, "tp", axis=0, tiled=True),
+        jnp.concatenate(
+            lax.all_to_all(jnp.stack([up_weight] * lax.axis_size("tp")), "tp", 0, 0), axis=0
+        ),
         lax.all_gather(down_weight.T, "tp", axis=0, tiled=True),
     )
     gate_pre = jnp.dot(rows_in, gate_full, preferred_element_type=jnp.float32)

time: 343 us -> 401 us (1.17)
  waiting for transfers between devices: 293 us -> 340 us
  starting transfers between devices: 0.23 us -> 6.68 us
  local copies, waits for them, and re-layouts: 1.09 us -> 5.43 us
    all_to_all x0 -> x1, waiting for transfers between devices: none -> 220 us  [per_device(): lax.all_to_all(jnp.stack([up_weight] * lax.axis_size('tp')), 'tp', 0, 0)]
    all_gather x1, waiting for transfers between devices: 63.3 us -> 0.01 us  [per_device(): lax.all_gather(gate_weight, 'tp', axis=0, tiled=True)]
    all_gather x1, waiting for transfers between devices: 55 us -> 0.01 us  [per_device(): lax.all_gather(down_weight.T, 'tp', axis=0, tiled=True)]
    all_gather x1 -> x0, waiting for transfers between devices: 54.6 us -> none  [per_device(): lax.all_gather(up_weight, 'tp', axis=0, tiled=True)]
    all_to_all x0 -> x1, starting transfers between devices: none -> 6.49 us  [per_device(): lax.all_to_all(jnp.stack([up_weight] * lax.axis_size('tp')), 'tp', 0, 0)]
    another operation x0 -> x1, local copies, waits for them, and re-layouts: none -> 4.03 us  [per_device(): jnp.stack([up_weight] * lax.axis_size('tp'))]
  transfers between devices with their start and end apart: 6 -> 6, of which waited for: 6 -> 4; matrix products, arithmetic and copies ran while one was open for 5% -> 6% of each run, Pallas kernels for 0% -> 0%
where the time goes in v1:
time: 401 us
  waiting for transfers between devices  340 us (85%)
  matrix products  32.3 us (8%)
  between operations  13.8 us (3%)
  starting transfers between devices  6.68 us (2%)
  local copies, waits for them, and re-layouts  5.43 us (1%)
    all_to_all x1, waiting for transfers between devices, per_device(): lax.all_to_all(jnp.stack([up_weight] * lax.axis_size('tp')), 'tp', 0, 0)  220 us
    reduce_scatter x1, waiting for transfers between devices, per_device(): lax.psum_scatter(partial_down.astype(jnp.bfloat16), 'tp', scatter_dimensi...  66.9 us
    reduce_scatter x1, waiting for transfers between devices, per_device(): lax.psum_scatter((contract_hidden(gate_grad, gate_full) + contract_hidden...  28.5 us
    all_gather x1, waiting for transfers between devices, per_device(): whole_grad = lax.all_gather(own_sum, 'fs', axis=0, tiled=True)  23.6 us
    dot_general x2, matrix products, contract_hidden(): lax.dot_general(left, right, (((1,), (1,)), ((), ())), preferred_element_...  8.49 us
  transfers between devices with their start and end apart: 6, of which 4 were waited for; matrix products, arithmetic and copies ran while one was open for 6% of the time, Pallas kernels for 0%

profile of v1, /device:TPU:0, one launch (start us, length us, event | category | flops | bytes accessed | tf_op | source)
XLA Modules:
  0.0 400.8 jit_solution(15408034538986337210)
XLA Ops:
  7.2 0.0 copy-start
  7.2 0.0 all-gather.6.cloned.1.call-start
  7.2 0.7 all-gather.6.cloned.1.call-update
  7.9 4.0 %stack.2 = bf16[8,256,1408]{2,1,0:T(8,128)(2,1)} broadcast(bf16[256,1408]{1,0:T(8,128)(2,1)} %param.8), dimensions={1,2} | broadcast | bytes 6488064 | tf_op jit(solution)/shard_map/stack | solution.py:27
  11.9 6.5 %all-to-all-start = ((bf16[8,256,1408]{2,1,0:T(8,128)(2,1)}), bf16[8,256,1408]{2,1,0:T(8,128)(2,1)}, u32[]{:S(2)}, u32[]{:S(2)}) async-start(bf16[8,256,1408]{2,1,0:T(8,128)(2,1)} %stack.2), calls=%async_computation | async-start | bytes 11534336 | tf_op jit(solution)/shard_map/all_to_all | solution.py:27
  18.4 0.0 all-gather.4.cloned.1.call-start
  18.5 0.7 all-gather.4.cloned.1.call-update
  19.2 0.0 reduce-scatter.3.cloned.1.call-start
  19.2 219.7 %all-to-all-done = bf16[8,256,1408]{2,1,0:T(8,128)(2,1)} async-done(((bf16[8,256,1408]{2,1,0:T(8,128)(2,1)}), bf16[8,256,1408]{2,1,0:T(8,128)(2,1)}, u32[]{:S(2)}, u32[]{:S(2)}) %all-to-all-start) | async-done | bytes 5767200 | tf_op jit(solution)/shard_map/all_to_all | solution.py:27
  238.9 0.0 copy-done.3
  238.9 6.1 %fusion.3 = f32[320,1408]{1,0:T(8,128)} fusion(bf16[2048,1408]{1,0:T(8,128)(2,1)} %bitcast.3, bf16[1,320,2048]{2,1,0:T(8,128)(2,1)S(1)} %copy-done.3), kind=kOutput, calls=%fused_computation.9 | convolution fusion | flops 1845493760 | bytes 8880128 | tf_op jit(solution)/shard_map/dot_general | solution.py:32
  245.0 6.0 %fusion.1 = f32[320,1408]{1,0:T(8,128)} fusion(bf16[2048,1408]{1,0:T(8,128)(2,1)} %all-gather.6.cloned.1.call-done, bf16[1,320,2048]{2,1,0:T(8,128)(2,1)S(1)} %copy-done.3), kind=kOutput, calls=%fused_computation.7 | convolution fusion | flops 1845493760 | bytes 8880128 | tf_op jit(solution)/shard_map/dot_general | solution.py:31
  251.1 0.0 copy-done
  251.1 0.0 copy-start.5
  251.1 5.0 %fusion.6 = f32[320,1408]{1,0:T(8,128)S(1)} fusion(bf16[2048,1408]{0,1:T(8,128)(2,1)} %all-gather.4.cloned.1.call-done, bf16[1,320,2048]{2,1,0:T(8,128)(2,1)S(1)} %copy-done), kind=kOutput, calls=%fused_computation.12 | convolution fusion | flops 1845493760 | bytes 8880128 | tf_op jit(solution)/shard_map/dot_general | solution.py:35
  256.1 0.0 copy-done.4
  256.1 0.0 copy-done.2
  256.1 0.3 copy-done.5
  256.4 2.5 fusion.8
  258.9 6.0 %fusion = bf16[320,2048]{1,0:T(8,128)(2,1)} fusion(f32[320,2048]{1,0:T(8,128)S(1)} %fusion.8, bf16[2048,1408]{1,0:T(8,128)(2,1)} %bitcast.3, f32[320,1408]{1,0:T(8,128)S(1)} %fusion.6, f32[320,1408]{1,0:T(8,128)S(1)} %copy-done.4), kind=kOutput, calls=%fused_computation.2 | convolution fusion | flops 1849507840 | bytes 13303808 | tf_op jit(solution)/shard_map/dot_general | solution.py:8
  264.9 0.0 reduce-scatter.3.cloned.1.call-update
  264.9 0.0 all-gather.8.cloned.1.call-start
  265.0 28.5 %reduce-scatter.3.cloned.1.call-done = bf16[80,2048]{1,0:T(8,128)(2,1)} async-done(((bf16[320,2048]{1,0:T(8,128)(2,1)}), bf16[80,2048]{1,0:T(8,128)(2,1)}) %reduce-scatter.3.cloned.1.call-update) | async-done | bytes 327696 | tf_op jit(solution)/shard_map/reduce_scatter | solution.py:42
  293.5 0.0 all-gather.8.cloned.1.call-update
  293.5 0.0 reduce-scatter.5.cloned.1.call-start
  293.6 6.7 %convolution_convert_fusion = bf16[1408,2048]{1,0:T(8,128)(2,1)} fusion(bf16[1,320,2048]{2,1,0:T(8,128)(2,1)S(1)} %copy-done, f32[320,1408]{1,0:T(8,128)} %fusion.3, f32[320,1408]{1,0:T(8,128)S(1)} %copy-done.4), kind=kOutput, calls=%fused_computation | convolution fusion | flops 1851080704 | bytes 10682368 | tf_op jit(solution)/shard_map/dot_general | solution.py:14
  300.3 0.0 reduce-scatter.5.cloned.1.call-update
  300.3 23.6 %all-gather.8.cloned.1.call-done = bf16[320,2048]{1,0:T(8,128)(2,1)} async-done(((bf16[80,2048]{1,0:T(8,128)(2,1)}), bf16[320,2048]{1,0:T(8,128)(2,1)}) %all-gather.8.cloned.1.call-update) | async-done | bytes 1310736 | tf_op jit(solution)/shard_map/all_gather | solution.py:50
  323.9 66.9 %reduce-scatter.5.cloned.1.call-done = bf16[1408,256]{1,0:T(8,128)(2,1)} async-done(((bf16[1408,2048]{1,0:T(8,128)(2,1)}), bf16[1408,256]{1,0:T(8,128)(2,1)}) %reduce-scatter.5.cloned.1.call-update) | async-done | bytes 720912 | tf_op jit(solution)/shard_map/reduce_scatter | solution.py:39
  390.9 2.3 convert_element_type.23
  393.2 0.0 copy-done.1
  393.2 1.1 copy.8
  (6 shorter events, 0.0 us)
Async XLA Ops:
  7.2 243.9 %copy-start = (bf16[1,320,2048]{2,1,0:T(8,128)(2,1)S(1)}, bf16[1,320,2048]{2,1,0:T(8,128)(2,1)}, u32[]{:S(2)}) copy-start(bf16[1,320,2048]{2,1,0:T(8,128)(2,1)} %param.6) | copy-start | bytes 3932164
  7.2 237.8 %all-gather.6.cloned.1.call-start = ((), (), s32[]{:S(2)}) async-start(), calls=%async_computation.4 | async-start | bytes 6488064 | tf_op jit(solution)/shard_map/all_gather | solution.py:25
  11.9 227.0 %copy-start.3 = (bf16[1,320,2048]{2,1,0:T(8,128)(2,1)S(1)}, bf16[1,320,2048]{2,1,0:T(8,128)(2,1)}, u32[]{:S(2)}) copy-start(bf16[1,320,2048]{2,1,0:T(8,128)(2,1)} %param.5) | copy-start | bytes 3932164
  11.9 227.0 %all-to-all-start = ((bf16[8,256,1408]{2,1,0:T(8,128)(2,1)}), bf16[8,256,1408]{2,1,0:T(8,128)(2,1)}, u32[]{:S(2)}, u32[]{:S(2)}) async-start(bf16[8,256,1408]{2,1,0:T(8,128)(2,1)} %stack.2), calls=%async_computation | async-start | bytes 11534336 | tf_op jit(solution)/shard_map/all_to_all | solution.py:27
  18.4 232.6 %all-gather.4.cloned.1.call-start = ((), (), s32[]{:S(2)}) async-start(), calls=%async_computation.3 | async-start | bytes 6488064 | tf_op jit(solution)/shard_map/all_gather | solution.py:29
  19.2 274.3 %reduce-scatter.3.cloned.1.call-start = ((), (), s32[]{:S(2)}) async-start(), calls=%async_computation.5 | async-start | bytes 1638400 | tf_op jit(solution)/shard_map/reduce_scatter | solution.py:42
  251.1 5.0 %copy-start.4 = (f32[320,1408]{1,0:T(8,128)S(1)}, f32[320,1408]{1,0:T(8,128)}, u32[]{:S(2)}) copy-start(f32[320,1408]{1,0:T(8,128)} %fusion.1) | copy-start | bytes 5406724
  251.1 5.0 %copy-start.2 = (bf16[2048,1408]{1,0:T(8,128)(2,1)S(1)}, bf16[2048,1408]{1,0:T(8,128)(2,1)}, u32[]{:S(2)}) copy-start(bf16[2048,1408]{1,0:T(8,128)(2,1)} %all-gather.6.cloned.1.call-done) | copy-start | bytes 17301508
  251.1 5.4 %copy-start.5 = (f32[320,1408]{1,0:T(8,128)S(1)}, f32[320,1408]{1,0:T(8,128)}, u32[]{:S(2)}) copy-start(f32[320,1408]{1,0:T(8,128)} %fusion.3) | copy-start | bytes 5406724
  264.9 59.0 %all-gather.8.cloned.1.call-start = ((), (), s32[]{:S(2)}) async-start(), calls=%async_computation.6 | async-start | bytes 1638400 | tf_op jit(solution)/shard_map/all_gather | solution.py:50
  293.5 97.3 %reduce-scatter.5.cloned.1.call-start = ((), (), s32[]{:S(2)}) async-start(), calls=%async_computation.7 | async-start | bytes 6488064 | tf_op jit(solution)/shard_map/reduce_scatter | solution.py:39
  323.9 69.3 %copy-start.1 = (bf16[320,2048]{1,0:T(8,128)(2,1)S(1)}, bf16[320,2048]{1,0:T(8,128)(2,1)}, u32[]{:S(2)}) copy-start(bf16[320,2048]{1,0:T(8,128)(2,1)} %all-gather.8.cloned.1.call-done) | copy-start | bytes 3932164
Sparse Core Ops, SparseCore 0:
  9.6 108.3 all-gather.5
  119.6 114.3 all-gather.3
  265.1 28.3 reduce-scatter.2
  295.2 28.6 all-gather.7
  326.1 64.7 reduce-scatter.4
